TPU v7x, 32 devices: a whole 2x2x4 slice. The times are simulated.
32 devices in a mesh: ep: 8 (over z, x), tp: 4 (over y, core).
Axes of the slice: x: 2, y: 2, z: 4, core: 2. Of those that a mesh axis runs over, the one named last changes fastest.
Arguments:
- tokens: bfloat16 [1024, 2048], P('ep'), may hold values from -6 to 6
- routing: int32 [1024, 2], P('ep'), may hold values from 0 to 7, all different within a row; in each aligned block of 128 rows (0 to 127, 128 to 255, ...) at most 56 rows name the same one
- router_weight: bfloat16 [2048, 8], replicated, may hold values from -0.125 to 0.125
- gate_weight: bfloat16 [8, 2048, 2048], P('ep', None, 'tp'), may hold values from -0.125 to 0.125
- up_weight: bfloat16 [8, 2048, 2048], P('ep', None, 'tp'), may hold values from -0.125 to 0.125
- down_weight: bfloat16 [8, 2048, 2048], P('ep', 'tp'), may hold values from -0.125 to 0.125
- cotangent: bfloat16 [1024, 2048], P('ep'), may hold values from -0.796875 to 0.796875
Outputs:
- token_grad: bfloat16 [1024, 2048], P('ep')
- router_grad: float32 [2048, 8], P('tp')
- router_rows: float32 [2048], P('tp')
- gate_grad: bfloat16 [8, 2048, 2048], P('ep', None, 'tp')
- up_grad: bfloat16 [8, 2048, 2048], P('ep', None, 'tp')
- down_grad: bfloat16 [8, 2048, 2048], P('ep', 'tp')
- gate_rows: float32 [8, 2048], P('ep')
- up_rows: float32 [8, 2048], P('ep')
- down_rows: float32 [8, 2048], P('ep', 'tp')
Inputs may be any that keep to these rules, and one draw needn't show every extreme that they name: `routing`: A row's 2 experts differ. Within the rows of one index of ep (128 rows), no expert is named more than 56 times, a bound that some block reaches.
All inputs are finite; a program needn't handle non-finite values.
Results may differ from a plain program's by a relative error of at most 0.01.
Values may be sent and summed in bfloat16 or wider, within the bound.
A program may use at most 64 MiB of HBM per device.

v0:
```python
import functools

import jax
import jax.numpy as jnp
from jax import lax
from jax.experimental import pallas as pl
from jax.experimental.pallas import tpu as pltpu
from jax.sharding import PartitionSpec as P

LANES = 128
F32 = jnp.float32
BF16 = jnp.bfloat16
ROWS_T = (((0,), (0,)), ((), ()))
COLS_T = (((1,), (1,)), ((), ()))


def barrier(n_ep, n_tp, me, tp):
    sem = pltpu.get_barrier_semaphore()
    for i in range(1, n_ep):
        pl.semaphore_signal(sem, inc=1, device_id={"ep": lax.rem(me + i, n_ep)})
    for i in range(1, n_tp):
        pl.semaphore_signal(sem, inc=1, device_id={"tp": lax.rem(tp + i, n_tp)})
    pl.semaphore_wait(sem, n_ep + n_tp - 2)


def remote(src, dst, send, recv, where):
    return pltpu.make_async_remote_copy(
        src_ref=src, dst_ref=dst, send_sem=send, recv_sem=recv, device_id=where
    )


def named_experts(routing, experts):
    ids = lax.broadcasted_iota(jnp.int32, (experts, routing.shape[1]), 0)
    named = jnp.zeros(ids.shape, F32)
    for k in range(routing.shape[0]):
        named = jnp.maximum(named, (routing[k : k + 1, :] == ids).astype(F32))
    return named.T


def column(value, index):
    ids = lax.broadcasted_iota(jnp.int32, value.shape, 1)
    return jnp.sum(jnp.where(ids == index, value, 0.0), axis=1, keepdims=True)


def lane_sum(value):
    total = value[:, :LANES]
    for at in range(LANES, value.shape[1], LANES):
        total = total + value[:, at : at + LANES]
    return total


def dispatch_kernel(
    dims, tok_ref, cot_ref, routing_ref, router_ref, w_gate, w_up, w_down,
    rows_out, cots_out, aff_ref, pos_ref, hidden_ref, gate_pre_ref, up_pre_ref, part_ref, term_ref,
    column_ref,
    rows_ref, cots_ref, scale_ref, gate_v, up_v, down_v, w_sem, flush_sem,
    stage, scale_stage, own_sem, sc_send, sc_recv, a_send, a_recv, y_send, y_recv, p_send, p_recv,
):
    n_ep, n_tp, n_batch, capacity, cap_pad, col_width = dims
    per = n_ep // n_batch
    n_y = n_tp // 2
    me = lax.axis_index("ep")
    tp = lax.axis_index("tp")
    y_at, core = tp // 2, lax.rem(tp, 2)
    partner = y_at * 2 + 1 - core
    experts = router_ref.shape[0]
    tok_count = tok_ref.shape[0]
    outs = (rows_ref, cots_ref)
    results = (rows_out, cots_out)
    weight_copies = [
        pltpu.make_async_copy(src.at[0], dst, w_sem.at[n])
        for n, (src, dst) in enumerate(((w_gate, gate_v), (w_up, up_v), (w_down, down_v)))
    ]
    for copy in weight_copies:
        copy.start()
    term_ref[...] = jnp.zeros_like(term_ref)

    def cols(index):
        return pl.ds(pl.multiple_of(index * col_width, LANES), col_width)

    named = named_experts(routing_ref[...], experts)
    below = (
        lax.broadcasted_iota(jnp.int32, (tok_count, tok_count), 1)
        < lax.broadcasted_iota(jnp.int32, (tok_count, tok_count), 0)
    ).astype(BF16)
    pos = jnp.dot(below, named.astype(BF16), preferred_element_type=F32)
    logits = lax.dot_general(tok_ref[...], router_ref[...], COLS_T, preferred_element_type=F32)
    aff = jax.nn.sigmoid(logits)
    total = jnp.sum(aff * named, axis=1, keepdims=True)
    weights = (aff * named / total).astype(BF16).astype(F32)
    aff_ref[...] = aff
    pos_ref[...] = pos
    token_cols = (tok_ref[:, cols(tp)], cot_ref[:, cols(tp)])
    slots = lax.broadcasted_iota(jnp.int32, (tok_count, cap_pad), 1).astype(F32)

    barrier(n_ep, n_tp, me, tp)
    for i in range(n_ep):
        dest = lax.rem(me + i, n_ep)
        pick = jnp.where(column(pos, dest) == slots, column(named, dest), 0.0)
        scale_stage[dest] = jnp.sum(pick * column(weights, dest), axis=0, keepdims=True)
        pick = pick.astype(BF16)
        for a in range(2):
            moved = lax.dot_general(pick, token_cols[a], ROWS_T, preferred_element_type=F32)
            stage[a, dest] = moved[:capacity].astype(BF16)
        for a in range(2):
            target = outs[a].at[me, :, cols(tp)]
            if i == 0:
                pltpu.make_async_copy(stage.at[a, dest], target, own_sem.at[a]).start()
            else:
                remote(
                    stage.at[a, dest], target, a_send.at[a, dest], a_recv.at[a, me], {"ep": dest}
                ).start()
        if i == 0:
            pltpu.make_async_copy(scale_stage.at[dest], scale_ref.at[me], own_sem.at[2]).start()
        else:
            remote(
                scale_stage.at[dest], scale_ref.at[me], sc_send.at[dest], sc_recv.at[me], {"ep": dest}
            ).start()

    def y_copy(a, batch, y_to):
        ref = outs[a].at[pl.ds(batch * per, per), :, cols(tp)]
        return remote(
            ref, ref, y_send.at[a, batch, y_to], y_recv.at[a, batch, y_at], {"tp": y_to * 2 + core}
        )

    def y_arrival(a, batch, y_from):
        ref = outs[a].at[pl.ds(batch * per, per), :, cols(y_from * 2 + core)]
        return remote(
            ref, ref, y_send.at[a, batch, y_from], y_recv.at[a, batch, y_from], {"tp": y_from * 2 + core}
        )

    def p_copy(a, batch, y_of):
        ref = outs[a].at[pl.ds(batch * per, per), :, cols(y_of * 2 + core)]
        return remote(ref, ref, p_send.at[a, batch, y_of], p_recv.at[a, batch, y_of], {"tp": partner})

    def p_arrival(a, batch, y_of):
        ref = outs[a].at[pl.ds(batch * per, per), :, cols(y_of * 2 + 1 - core)]
        return remote(ref, ref, p_send.at[a, batch, y_of], p_recv.at[a, batch, y_of], {"tp": partner})

    def relay(batch):
        for a in range(2):
            for j in range(1, n_y):
                y_from = lax.rem(y_at + j, n_y)
                y_arrival(a, batch, y_from).wait_recv()
                p_copy(a, batch, y_from).start()

    my_batch = me // per

    def batch_at(i):
        return lax.rem(my_batch - i + 2 * n_batch, n_batch)

    def flush(a, batch):
        part = pl.ds(batch * per, per)
        return pltpu.make_async_copy(outs[a].at[part], results[a].at[part], flush_sem.at[a, batch])

    def arrive(batch):
        for a in range(2):
            for j in range(per):
                source = batch * per + j

                @pl.when(source == me)
                def _(a=a, source=source):
                    pltpu.make_async_copy(
                        stage.at[a, source], outs[a].at[source, :, cols(tp)], own_sem.at[a]
                    ).wait()

                @pl.when(source != me)
                def _(a=a, source=source):
                    ref = outs[a].at[source, :, cols(tp)]
                    remote(
                        ref, ref, a_send.at[a, source], a_recv.at[a, source], {"ep": source}
                    ).wait_recv()

            for j in range(1, n_y):
                y_copy(a, batch, lax.rem(y_at + j, n_y)).start()
            p_copy(a, batch, y_at).start()

    def compute(source):
        @pl.when(source == me)
        def _():
            pltpu.make_async_copy(scale_stage.at[source], scale_ref.at[source], own_sem.at[2]).wait()

        @pl.when(source != me)
        def _():
            ref = scale_ref.at[source]
            remote(ref, ref, sc_send.at[source], sc_recv.at[source], {"ep": source}).wait_recv()

        scale = jnp.broadcast_to(scale_ref[source], (8, cap_pad)).T[:capacity, 0:1]
        column_ref[source] = scale
        rows_in, cots_in = rows_ref[source], cots_ref[source]
        pre_gate = jnp.dot(rows_in, gate_v[...], preferred_element_type=F32)
        pre_up = jnp.dot(rows_in, up_v[...], preferred_element_type=F32)
        back = lax.dot_general(cots_in, down_v[...], COLS_T, preferred_element_type=F32)
        sig = jax.nn.sigmoid(pre_gate)
        hidden = (pre_gate * sig * pre_up).astype(BF16)
        hidden_ref[source] = hidden
        terms = lane_sum(hidden.astype(F32) * back)
        term_ref[source, :, :capacity] = jnp.sum(terms.T, axis=0, keepdims=True)
        scaled = scale * back
        grad_up = (scaled * pre_gate * sig).astype(BF16)
        grad_gate = (scaled * pre_up * sig * (1.0 + pre_gate * (1.0 - sig))).astype(BF16)
        up_pre_ref[source] = grad_up
        gate_pre_ref[source] = grad_gate
        part = lax.dot_general(grad_gate, gate_v[...], COLS_T, preferred_element_type=F32)
        part = part + lax.dot_general(grad_up, up_v[...], COLS_T, preferred_element_type=F32)
        part_ref[source] = part.astype(BF16)

    for copy in weight_copies:
        copy.wait()

    def step(i, carry):
        @pl.when(i < n_batch)
        def _():
            arrive(batch_at(i))

        @pl.when((i >= 1) & (i < n_batch + 1))
        def _():
            relay(batch_at(i - 1))

        @pl.when(i >= 2)
        def _():
            batch = batch_at(i - 2)
            for a in range(2):
                for j in range(n_y):
                    p_arrival(a, batch, lax.rem(y_at + j, n_y)).wait_recv()
                flush(a, batch).start()
            for j in range(per):
                compute(batch * per + j)

        return carry

    lax.fori_loop(0, n_batch + 2, step, 0)
    batches = range(n_batch)
    for i in range(1, n_ep):
        other = lax.rem(me + i, n_ep)
        remote(
            scale_stage.at[other], scale_ref.at[other], sc_send.at[other], sc_recv.at[other], {"ep": other}
        ).wait_send()
        for a in range(2):
            remote(
                stage.at[a, other], outs[a].at[me, :, cols(tp)], a_send.at[a, other],
                a_recv.at[a, me], {"ep": other},
            ).wait_send()
    for batch in batches:
        for a in range(2):
            flush(a, batch).wait()
            for j in range(n_y):
                y_to = lax.rem(y_at + j, n_y)
                if j > 0:
                    y_copy(a, batch, y_to).wait_send()
                p_copy(a, batch, y_to).wait_send()


def combine_kernel(
    dims, part_ref, gate_ref, rowsq_ref, tok_ref, routing_ref, router_ref, aff_ref, pos_ref,
    token_ref, rgrad_ref, rowsum_ref,
    r1, s1, r2, res, back, gate_in, gate_sum, gate_back, rowsq_in, rpart, rparts, tgrad,
    s1_send, s1_recv, s2_send, s2_recv, s3_send, s3_recv, gt_send, gt_recv, gb_send, gb_recv,
    rs_send, rs_recv, rp_send, rp_recv, ty_send, ty_recv, tp_send, tp_recv, own_sem,
):
    n_ep, n_tp, n_batch, capacity, cap_pad, col_width = dims
    per = n_ep // n_batch
    n_y = n_tp // 2
    me = lax.axis_index("ep")
    tp = lax.axis_index("tp")
    y_at, core = tp // 2, lax.rem(tp, 2)
    partner = y_at * 2 + 1 - core
    experts = router_ref.shape[0]
    tok_count = tok_ref.shape[0]

    def cols(index):
        return pl.ds(pl.multiple_of(index * col_width, LANES), col_width)

    def span(batch):
        return pl.ds(batch * per, per)

    my_batch = me // per
    batches = [lax.rem(my_batch + i + 1, n_batch) for i in range(n_batch)]
    barrier(n_ep, n_tp, me, tp)

    def first(batch, y_to):
        return remote(
            part_ref.at[span(batch), :, cols(y_to * 2 + 1 - core)], r1.at[y_to, span(batch)],
            s1_send.at[batch, y_to], s1_recv.at[batch, y_to], {"tp": partner},
        )

    def second(batch, y_to, y_from):
        return remote(
            s1.at[y_to, span(batch)], r2.at[y_from, span(batch)],
            s2_send.at[batch, y_to], s2_recv.at[batch, y_from], {"tp": y_to * 2 + core},
        )

    def third(dest, source):
        return remote(
            res.at[dest], back.at[source], s3_send.at[dest], s3_recv.at[source], {"ep": dest}
        )

    def gate_part(other, slot):
        return remote(gate_ref, gate_in.at[slot], gt_send.at[other], gt_recv.at[slot], {"tp": other})

    def gate_home(dest, source):
        return remote(
            gate_sum.at[dest], gate_back.at[source], gb_send.at[dest], gb_recv.at[source], {"ep": dest}
        )

    def squares(other, slot):
        return remote(rowsq_ref, rowsq_in.at[slot], rs_send.at[other], rs_recv.at[slot], {"tp": other})

    for i in range(1, n_tp):
        gate_part(lax.rem(tp + i, n_tp), tp).start()
    for batch in batches:
        for j in range(n_y):
            first(batch, lax.rem(y_at + n_y - 1 - j, n_y)).start()
    for i in range(1, n_tp):
        squares(lax.rem(tp + i, n_tp), tp).start()

    def reduce_core(batch):
        for j in range(n_y):
            y_to = lax.rem(y_at + n_y - 1 - j, n_y)
            first(batch, y_to).wait_recv()
            mine = part_ref[span(batch), :, cols(y_to * 2 + core)].astype(F32)
            s1[y_to, span(batch)] = (mine + r1[y_to, span(batch)].astype(F32)).astype(BF16)
            if j < n_y - 1:
                second(batch, y_to, y_at).start()

    def reduce_y(batch, is_own):
        total = s1[y_at, span(batch)].astype(F32)
        for j in range(1, n_y):
            y_from = lax.rem(y_at + j, n_y)
            second(batch, y_from, y_from).wait_recv()
            total = total + r2[y_from, span(batch)].astype(F32)
        res[span(batch)] = total.astype(BF16)
        for j in range(per):
            dest = batch * per + j

            def to_self(dest=dest):
                pltpu.make_async_copy(res.at[dest], back.at[dest], own_sem.at[0]).start()

            def to_other(dest=dest):
                third(dest, me).start()

            if per == 1:
                (to_self if is_own else to_other)()
            elif not is_own:
                to_other()
            else:
                pl.when(dest == me)(to_self)
                pl.when(dest != me)(to_other)

    for i, batch in enumerate(batches):
        reduce_core(batch)
        if i == 1:
            gate = gate_ref[...]
            for j in range(1, n_tp):
                other = lax.rem(tp + j, n_tp)
                gate_part(other, other).wait_recv()
                gate = gate + gate_in[other]
            gate_sum[...] = gate
            for j in range(1, n_ep):
                gate_home(lax.rem(me + j, n_ep), me).start()
        if i > 1:
            reduce_y(batches[i - 2], False)
    reduce_y(batches[-2], n_batch == 1)
    reduce_y(batches[-1], True)

    named = named_experts(routing_ref[...], experts)
    aff, pos = aff_ref[...], pos_ref[...]
    total = jnp.sum(aff * named, axis=1, keepdims=True)
    weights = aff * named / total
    slots = lax.broadcasted_iota(jnp.int32, (tok_count, cap_pad), 1).astype(F32)
    ids = lax.broadcasted_iota(jnp.int32, (tok_count, experts), 1)

    d_weights = jnp.zeros((tok_count, experts), F32)
    picks = []
    for i in range(n_ep):
        source = lax.rem(me + i, n_ep)
        if i == 0:
            terms = gate_sum[source]
        else:
            gate_home(source, source).wait_recv()
            terms = gate_back[source]
        terms = terms.astype(BF16).astype(F32)
        pick = jnp.where(column(pos, source) == slots, column(named, source), 0.0)
        term = jnp.sum(pick * terms, axis=1, keepdims=True)
        d_weights = jnp.where(ids == source, term, d_weights)
        picks.append(pick.astype(BF16))
    mean = jnp.sum(d_weights * weights, axis=1, keepdims=True)
    d_logits = ((d_weights - mean) / total * aff * (1.0 - aff) * named).astype(BF16)

    rpart[...] = lax.dot_general(d_logits, tok_ref[:, cols(tp)], ROWS_T, preferred_element_type=F32)

    def router_copy(dest, source):
        return remote(rpart, rparts.at[source], rp_send.at[dest], rp_recv.at[source], {"ep": dest})

    for i in range(1, n_ep):
        router_copy(lax.rem(me + i, n_ep), me).start()

    grad = jnp.dot(d_logits, router_ref[:, cols(tp)], preferred_element_type=F32)
    for i in range(n_ep):
        source = lax.rem(me - i + n_ep, n_ep)
        if i == 0:
            pltpu.make_async_copy(res.at[me], back.at[me], own_sem.at[0]).wait()
        else:
            third(source, source).wait_recv()
        pick = picks[(n_ep - i) % n_ep][:, :capacity]
        grad = grad + jnp.dot(pick, back[source], preferred_element_type=F32)
    tgrad[...] = grad.astype(BF16)

    def to_y(y_to):
        return remote(
            tgrad, token_ref.at[:, cols(tp)], ty_send.at[y_to], ty_recv.at[y_at], {"tp": y_to * 2 + core}
        )

    def from_y(y_from):
        ref = token_ref.at[:, cols(y_from * 2 + core)]
        return remote(ref, ref, ty_send.at[y_from], ty_recv.at[y_from], {"tp": y_from * 2 + core})

    def own_pair():
        return remote(
            tgrad, token_ref.at[:, cols(tp)], tp_send.at[y_at], tp_recv.at[y_at], {"tp": partner}
        )

    def pair(y_of):
        ref = token_ref.at[:, cols(y_of * 2 + core)]
        return remote(ref, ref, tp_send.at[y_of], tp_recv.at[y_of], {"tp": partner})

    def pair_in(y_of):
        ref = token_ref.at[:, cols(y_of * 2 + 1 - core)]
        return remote(ref, ref, tp_send.at[y_of], tp_recv.at[y_of], {"tp": partner})

    for j in range(1, n_y):
        to_y(lax.rem(y_at + j, n_y)).start()
    own_pair().start()
    own = pltpu.make_async_copy(tgrad, token_ref.at[:, cols(tp)], own_sem.at[1])
    own.start()

    rgrad = rpart[...]
    for i in range(1, n_ep):
        source = lax.rem(me + i, n_ep)
        router_copy(source, source).wait_recv()
        rgrad = rgrad + rparts[source]
    rgrad_ref[...] = rgrad
    sums = rowsq_ref[...]
    for i in range(1, n_tp):
        other = lax.rem(tp + i, n_tp)
        squares(other, other).wait_recv()
        sums = sums + rowsq_in[other]
    rowsum_ref[...] = sums

    for j in range(1, n_y):
        y_from = lax.rem(y_at + j, n_y)
        from_y(y_from).wait_recv()
        pair(y_from).start()
    for j in range(n_y):
        pair_in(lax.rem(y_at + j, n_y)).wait_recv()
    own.wait()
    own_pair().wait_send()
    for j in range(1, n_y):
        other = lax.rem(y_at + j, n_y)
        to_y(other).wait_send()
        pair(other).wait_send()
    for i in range(1, n_tp):
        other = lax.rem(tp + i, n_tp)
        gate_part(other, tp).wait_send()
        squares(other, tp).wait_send()
    for i in range(1, n_ep):
        other = lax.rem(me + i, n_ep)
        gate_home(other, me).wait_send()
        third(other, me).wait_send()
        router_copy(other, me).wait_send()
    for batch in batches:
        for j in range(n_y):
            y_to = lax.rem(y_at + j, n_y)
            first(batch, y_to).wait_send()
            if j > 0:
                second(batch, y_to, y_at).wait_send()


def weight_grad_kernel(
    rows_ref, cots_ref, hidden_ref, gate_ref, up_ref, scale_ref,
    gate_out, up_out, down_out, squares_out, down_squares_out, hidden_t, down_acc,
):
    step = pl.program_id(0)

    @pl.when(step == 0)
    def _():
        hidden_t[...] = hidden_ref[...].T
        down_acc[...] = jnp.zeros_like(down_acc)

    rows_t = rows_ref[...].T
    for a, (pre, out) in enumerate(((gate_ref, gate_out), (up_ref, up_out))):
        grad = jnp.dot(rows_t, pre[...], preferred_element_type=F32)
        out[...] = grad.astype(BF16)
        squares_out[a] = jnp.sum(lane_sum(grad * grad).T, axis=0, keepdims=True)
    weighted = (scale_ref[...] * cots_ref[...].astype(F32)).astype(BF16)
    grad = jnp.dot(hidden_t[...], weighted, preferred_element_type=F32)
    down_out[...] = grad.astype(BF16)
    down_acc[...] += lane_sum(grad * grad)

    @pl.when(step == pl.num_programs(0) - 1)
    def _():
        down_squares_out[...] = jnp.sum(down_acc[...].T, axis=0, keepdims=True)


def finish_kernel(token_ref, router_ref, sums_ref, token_out, router_out, rows_out, gate_out, up_out):
    token_out[...] = token_ref[...]
    grad = router_ref[...]
    router_out[...] = grad
    rows_out[...] = jnp.sum(grad * grad, axis=0, keepdims=True)
    gate_out[...] = sums_ref[0]
    up_out[...] = sums_ref[1]


def per_device(tokens, routing, router_weight, gate_weight, up_weight, down_weight, cotangent):
    n_ep = lax.axis_size("ep")
    n_tp = lax.axis_size("tp")
    tok_count, width = tokens.shape
    top_count = routing.shape[1]
    experts = router_weight.shape[1]
    capacity = 7 * tok_count * top_count // (4 * experts)
    cap_pad = -(-capacity // LANES) * LANES
    slots = n_ep * capacity
    col_width = width // n_tp
    n_batch = min(n_ep, 8)
    n_y = n_tp // 2
    dims = (n_ep, n_tp, n_batch, capacity, cap_pad, col_width)
    vmem = pl.BlockSpec(memory_space=pltpu.VMEM)
    hbm = pl.BlockSpec(memory_space=pl.ANY)
    dma = pltpu.SemaphoreType.DMA

    units = gate_weight.shape[2]

    def per_slot(size, dtype):
        return jax.ShapeDtypeStruct((n_ep, capacity, size), dtype)

    (rows, cots, aff, pos, hidden, grad_gate_pre, grad_up_pre, partial_value, gate_term,
     slot_scale) = pl.pallas_call(
        functools.partial(dispatch_kernel, dims),
        out_shape=(
            per_slot(width, BF16),
            per_slot(width, BF16),
            jax.ShapeDtypeStruct((tok_count, experts), F32),
            jax.ShapeDtypeStruct((tok_count, experts), F32),
            per_slot(units, BF16),
            per_slot(units, BF16),
            per_slot(units, BF16),
            per_slot(width, BF16),
            jax.ShapeDtypeStruct((n_ep, 1, cap_pad), F32),
            per_slot(1, F32),
        ),
        in_specs=[vmem] * 4 + [hbm] * 3,
        out_specs=(hbm, hbm) + (vmem,) * 8,
        scratch_shapes=[
            pltpu.VMEM((n_ep, capacity, width), BF16),
            pltpu.VMEM((n_ep, capacity, width), BF16),
            pltpu.VMEM((n_ep, 1, cap_pad), F32),
            pltpu.VMEM((width, units), BF16),
            pltpu.VMEM((width, units), BF16),
            pltpu.VMEM((units, width), BF16),
            dma((3,)), dma((2, n_batch)),
            pltpu.VMEM((2, n_ep, capacity, col_width), BF16),
            pltpu.VMEM((n_ep, 1, cap_pad), F32),
            dma((3,)),
            dma((n_ep,)), dma((n_ep,)),
            dma((2, n_ep)), dma((2, n_ep)),
            dma((2, n_batch, n_y)), dma((2, n_batch, n_y)),
            dma((2, n_batch, n_y)), dma((2, n_batch, n_y)),
        ],
        compiler_params=pltpu.CompilerParams(collective_id=0, has_side_effects=True),
        name="dispatch",
    )(tokens, cotangent, routing.T, router_weight.T, gate_weight, up_weight, down_weight)

    rows, cots, hidden, grad_gate_pre, grad_up_pre, slot_scale = (
        value.reshape(slots, -1)
        for value in (rows, cots, hidden, grad_gate_pre, grad_up_pre, slot_scale)
    )
    span = 2 * LANES if width % (2 * LANES) == 0 else LANES
    whole = pl.BlockSpec((slots, units), lambda i: (0, 0))
    grad_gate, grad_up, grad_down, row_squares, down_rows = pl.pallas_call(
        weight_grad_kernel,
        grid=(width // span,),
        out_shape=(
            jax.ShapeDtypeStruct((width, units), BF16),
            jax.ShapeDtypeStruct((width, units), BF16),
            jax.ShapeDtypeStruct((units, width), BF16),
            jax.ShapeDtypeStruct((2, 1, width), F32),
            jax.ShapeDtypeStruct((1, units), F32),
        ),
        in_specs=[
            pl.BlockSpec((slots, span), lambda i: (0, i)),
            pl.BlockSpec((slots, span), lambda i: (0, i)),
            whole, whole, whole,
            pl.BlockSpec((slots, 1), lambda i: (0, 0)),
        ],
        out_specs=(
            pl.BlockSpec((span, units), lambda i: (i, 0)),
            pl.BlockSpec((span, units), lambda i: (i, 0)),
            pl.BlockSpec((units, span), lambda i: (0, i)),
            pl.BlockSpec((2, 1, span), lambda i: (0, 0, i)),
            pl.BlockSpec((1, units), lambda i: (0, 0)),
        ),
        scratch_shapes=[pltpu.VMEM((units, slots), BF16), pltpu.VMEM((units, LANES), F32)],
        compiler_params=pltpu.CompilerParams(dimension_semantics=("arbitrary",)),
        name="weight_grads",
    )(rows, cots, hidden, grad_gate_pre, grad_up_pre, slot_scale)

    token_grad, router_grad, row_sums = pl.pallas_call(
        functools.partial(combine_kernel, dims),
        out_shape=(
            jax.ShapeDtypeStruct((tok_count, width), BF16),
            jax.ShapeDtypeStruct((experts, col_width), F32),
            jax.ShapeDtypeStruct(row_squares.shape, F32),
        ),
        in_specs=[vmem] * 8,
        out_specs=(hbm, vmem, vmem),
        scratch_shapes=[
            pltpu.VMEM((n_y, n_ep, capacity, col_width), BF16),
            pltpu.VMEM((n_y, n_ep, capacity, col_width), BF16),
            pltpu.VMEM((n_y, n_ep, capacity, col_width), BF16),
            pltpu.VMEM((n_ep, capacity, col_width), BF16),
            pltpu.VMEM((n_ep, capacity, col_width), BF16),
            pltpu.VMEM((n_tp, n_ep, 1, cap_pad), F32),
            pltpu.VMEM((n_ep, 1, cap_pad), F32),
            pltpu.VMEM((n_ep, 1, cap_pad), F32),
            pltpu.VMEM((n_tp,) + row_squares.shape, F32),
            pltpu.VMEM((experts, col_width), F32),
            pltpu.VMEM((n_ep, experts, col_width), F32),
            pltpu.VMEM((tok_count, col_width), BF16),
            dma((n_batch, n_y)), dma((n_batch, n_y)),
            dma((n_batch, n_y)), dma((n_batch, n_y)),
            dma((n_ep,)), dma((n_ep,)),
            dma((n_tp,)), dma((n_tp,)),
            dma((n_ep,)), dma((n_ep,)),
            dma((n_tp,)), dma((n_tp,)),
            dma((n_ep,)), dma((n_ep,)),
            dma((n_y,)), dma((n_y,)),
            dma((n_y,)), dma((n_y,)),
            dma((2,)),
        ],
        compiler_params=pltpu.CompilerParams(collective_id=1, has_side_effects=True),
        name="combine",
    )(partial_value, gate_term, row_squares, tokens,
      routing.T, router_weight.T, aff, pos)

    token_grad, router_grad, router_rows, gate_rows, up_rows = pl.pallas_call(
        finish_kernel,
        out_shape=(
            jax.ShapeDtypeStruct((tok_count, width), BF16),
            jax.ShapeDtypeStruct((experts, col_width), F32),
            jax.ShapeDtypeStruct((1, col_width), F32),
            jax.ShapeDtypeStruct((1, width), F32),
            jax.ShapeDtypeStruct((1, width), F32),
        ),
        in_specs=[vmem] * 3,
        out_specs=(vmem,) * 5,
        name="finish",
    )(token_grad, router_grad, row_sums)
    return (
        token_grad,
        router_grad.T,
        router_rows[0],
        grad_gate[None],
        grad_up[None],
        grad_down[None],
        gate_rows,
        up_rows,
        down_rows,
    )


def solution(mesh):
    return jax.shard_map(
        per_device,
        mesh=mesh,
        in_specs=(
            P("ep", None),
            P("ep", None),
            P(),
            P("ep", None, "tp"),
            P("ep", None, "tp"),
            P("ep", "tp", None),
            P("ep", None),
        ),
        out_specs=(
            P("ep", None),
            P("tp", None),
            P("tp"),
            P("ep", None, "tp"),
            P("ep", None, "tp"),
            P("ep", "tp", None),
            P("ep", None),
            P("ep", None),
            P("ep", "tp"),
        ),
        check_vma=False,
    )
```

profile of v0, /device:TPU:0, one launch (start us, length us, event | category | flops | bytes accessed | tf_op | source)
XLA Modules:
  0.0 97.2 jit_solution(5025842412385463682)
XLA Ops:
  0.6 50.0 %dispatch.1 = (bf16[8,56,2048]{2,1,0:T(8,128)(2,1)}, bf16[8,56,2048]{2,1,0:T(8,128)(2,1)}, f32[128,8]{1,0:T(8,128)}, f32[128,8]{1,0:T(8,128)}, bf16[8,56,512]{2,...) custom-call(bf16[128,2048]{1,0:T(8,128)(2,1)} %tok_ref.3, ...), custom_call_target="tpu_custom_call" | custom-call | tf_op jit(solution)/shard_map/dispatch/pallas_call | solution.py:537
  50.6 10.3 %weight_grads.1 = (bf16[2048,512]{1,0:T(8,128)(2,1)}, bf16[2048,512]{1,0:T(8,128)(2,1)}, bf16[512,2048]{1,0:T(8,128)(2,1)}, f32[2,1,2048]{2,1,0:T(1,128)}, f32[1,512]{1,0:T(1,128)}) custom-call(bf16[448,2048]{1,0:T(8,128)(2,1)} %bitcast.13, bf16[448,2048]{1,0:T(8,128)(2,1)} %bitcast.14, bf16[448,512]{1,0:T(8,128)(2,1)} %bitcast.15, ...), custom_call_target="tpu_custom_call" | custom-call | tf_op jit(solution)/shard_map/weight_grads/pallas_call | solution.py:579
  60.9 34.4 %combine.1 = (bf16[128,2048]{1,0:T(8,128)(2,1)}, f32[8,512]{1,0:T(8,128)}, f32[2,1,2048]{2,1,0:T(1,128)}) custom-call(bf16[8,56,2048]{2,1,0:T(8,128)(2,1)} %get-tuple-element.32.part_ref, f32[8,1,128]{2,1,0:T(1,128)} %get-tuple-element.33.gate_ref, f32[2,1,2048]{2,1,0:T(1,128)} %get-tuple-element.40.rowsq_ref, bf16[128,2048]{1,0:T(8,128)(2,1)} %tok_ref.3, ...), custom_call_target="tpu_custom_call" | custom-call | tf_op jit(solution)/shard_map/combine/pallas_call | solution.py:607
  95.3 1.9 %finish.1 = (bf16[128,2048]{1,0:T(8,128)(2,1)}, f32[8,512]{1,0:T(8,128)}, f32[1,512]{1,0:T(1,128)}, f32[1,2048]{1,0:T(1,128)}, f32[1,2048]{1,0:T(1,128)}) custom-call(bf16[128,2048]{1,0:T(8,128)(2,1)} %get-tuple-element.43.token_ref, f32[8,512]{1,0:T(8,128)} %get-tuple-element.44.router_ref, f32[2,1,2048]{2,1,0:T(1,128)} %get-tuple-element.45.sums_ref), custom_call_target="tpu_custom_call" | custom-call | tf_op jit(solution)/shard_map/finish/pallas_call | solution.py:645
where the time goes:
time: 98.8 us; the launch traced here: 97.2 us
  Pallas kernels  96.5 us (98%)
    pallas_call x1, Pallas kernels, per_device(): pl.pallas_call(functools.partial(dispatch_kernel, dims), out_shape=(per_s...  50 us
    pallas_call x1, Pallas kernels, per_device(): pl.pallas_call(functools.partial(combine_kernel, dims), out_shape=(jax.Sh...  34.4 us
    pallas_call x1, Pallas kernels, per_device(): pl.pallas_call(weight_grad_kernel, grid=(width // span,), out_shape=(jax....  10.3 us

commit v1 on v0

v1 whole, which is shorter than its diff:
```python
import functools

import jax
import jax.numpy as jnp
from jax import lax
from jax.experimental import pallas as pl
from jax.experimental.pallas import tpu as pltpu
from jax.sharding import PartitionSpec as P

LANES = 128
F32 = jnp.float32
BF16 = jnp.bfloat16
ROWS_T = (((0,), (0,)), ((), ()))
COLS_T = (((1,), (1,)), ((), ()))


def barrier(n_ep, n_tp, me, tp):
    sem = pltpu.get_barrier_semaphore()
    for i in range(1, n_ep):
        pl.semaphore_signal(sem, inc=1, device_id={"ep": lax.rem(me + i, n_ep)})
    for i in range(1, n_tp):
        pl.semaphore_signal(sem, inc=1, device_id={"tp": lax.rem(tp + i, n_tp)})
    pl.semaphore_wait(sem, n_ep + n_tp - 2)


def remote(src, dst, send, recv, where):
    return pltpu.make_async_remote_copy(
        src_ref=src, dst_ref=dst, send_sem=send, recv_sem=recv, device_id=where
    )


def lane_sum(value):
    total = value[:, :LANES]
    for at in range(LANES, value.shape[1], LANES):
        total = total + value[:, at : at + LANES]
    return total


def flip(index, step):
    out, bit = index, 1
    while bit <= step:
        if step & bit:
            out = out + bit - 2 * bit * lax.rem(index // bit, 2)
        bit *= 2
    return out


def moe_kernel(
    dims, tok_ref, cot_ref, routing_ref, router_ref, w_gate, w_up, w_down,
    token_ref, rgrad_ref, rowsum_ref, gate_out, up_out, down_out, down_rows_ref,
    x_ref, z_ref, scale_ref, gate_v, up_v, down_v, gate_t, up_t, down_t, w_sem,
    stage, scale_stage, pick_ref, pos_ref, weight_ref,
    xt_ref, ht_ref, weighted_ref, gate_pre_ref, up_pre_ref, part_ref, term_ref, down_acc,
    r1, s1, r2, res, back, gate_in, gate_sum, gate_back, rowsq_ref, rowsq_in, rpart, rparts, tgrad,
    sc_send, sc_recv, a_send, a_recv, y_send, y_recv, p_send, p_recv,
    s1_send, s1_recv, s2_send, s2_recv, s3_send, s3_recv, gt_send, gt_recv, gb_send, gb_recv,
    rs_send, rs_recv, rp_send, rp_recv, ty_send, ty_recv, tp_send, tp_recv,
):
    n_ep, n_tp, n_batch, sent, slab, col_width, span = dims
    per = n_ep // n_batch
    rows = per * slab
    n_y = n_tp // 2
    me = lax.axis_index("ep")
    tp = lax.axis_index("tp")
    y_at, core = tp // 2, lax.rem(tp, 2)
    partner = y_at * 2 + 1 - core
    experts = router_ref.shape[0]
    tok_count, width = tok_ref.shape
    units = gate_v.shape[1]
    ins = (tok_ref, cot_ref)
    outs = (x_ref, z_ref)
    peers = [flip(me, i) for i in range(n_ep)]
    others_y = [lax.rem(y_at + j, n_y) for j in range(1, n_y)]
    others_tp = [lax.rem(tp + j, n_tp) for j in range(1, n_tp)]

    sem = pltpu.get_barrier_semaphore()
    for i in range(1, n_ep):
        pl.semaphore_signal(sem, inc=1, device_id={"ep": peers[i]})
    for other in others_tp:
        pl.semaphore_signal(sem, inc=1, device_id={"tp": other})
    weight_copies = [
        pltpu.make_async_copy(src.at[0], dst, w_sem.at[n])
        for n, (src, dst) in enumerate(((w_gate, gate_v), (w_up, up_v), (w_down, down_v)))
    ]
    for copy in weight_copies:
        copy.start()

    def cols(index):
        return pl.ds(pl.multiple_of(index * col_width, LANES), col_width)

    routing = routing_ref[...]
    expert_ids = lax.broadcasted_iota(jnp.int32, (experts, tok_count), 0)
    named = jnp.zeros((experts, tok_count), F32)
    for k in range(routing.shape[0]):
        named = jnp.maximum(named, (routing[k : k + 1, :] == expert_ids).astype(F32))
    earlier = (
        lax.broadcasted_iota(jnp.int32, (tok_count, tok_count), 0)
        < lax.broadcasted_iota(jnp.int32, (tok_count, tok_count), 1)
    ).astype(BF16)
    pos = jnp.dot(named.astype(BF16), earlier, preferred_element_type=F32)
    pos_ref[...] = jnp.where(named > 0.0, pos, -1.0)
    slot_ids = lax.broadcasted_iota(jnp.int32, (slab, tok_count), 0).astype(F32)

    def pick_rows(i):
        pick = (pos_ref[pl.ds(peers[i], 1), :] == slot_ids).astype(F32).astype(BF16)
        pick_ref[i // per, (i % per) * slab : (i % per + 1) * slab, :] = pick
        return pick

    def a_copy(a, i):
        return remote(
            stage.at[a, i, pl.ds(0, sent)], outs[a].at[i, pl.ds(0, sent), cols(tp)],
            a_send.at[a, i], a_recv.at[a, i], {"ep": peers[i]},
        )

    def sc_copy(i):
        return remote(scale_stage.at[i], scale_ref.at[i], sc_send.at[i], sc_recv.at[i], {"ep": peers[i]})

    token_cols = (tok_ref[:, cols(tp)], cot_ref[:, cols(tp)])
    for i in range(1, n_ep):
        pick = pick_rows(i)
        for a in range(2):
            stage[a, i] = jnp.dot(pick, token_cols[a], preferred_element_type=F32).astype(BF16)
        if i == 1:
            pl.semaphore_wait(sem, n_ep + n_tp - 2)
        for a in range(2):
            a_copy(a, i).start()
    pick = pick_rows(0)
    for a in range(2):
        outs[a][0] = jnp.dot(pick, ins[a][...], preferred_element_type=F32).astype(BF16)
        if slab > sent:
            for i in range(1, n_ep):
                outs[a][i, sent:, :] = jnp.zeros((slab - sent, width), BF16)
    if slab > sent:
        for i in range(n_ep):
            back[i, sent:, :] = jnp.zeros((slab - sent, col_width), BF16)

    logits = lax.dot_general(router_ref[...], tok_ref[...], COLS_T, preferred_element_type=F32)
    aff = jax.nn.sigmoid(logits)
    total = jnp.sum(aff * named, axis=0, keepdims=True)
    weights = aff * named / total
    weight_ref[...] = weights.astype(BF16).astype(F32)
    lanes = lax.broadcasted_iota(jnp.int32, (1, rows), 1)

    def mine_of(i):
        return (lanes >= (i % per) * slab) & (lanes < (i % per + 1) * slab)

    for i in range(n_ep):
        row = jnp.broadcast_to(weight_ref[pl.ds(peers[i], 1), :], (8, tok_count)).astype(BF16)
        scale = lax.dot_general(row, pick_ref[i // per], COLS_T, preferred_element_type=F32)
        scale = jnp.where(mine_of(i), scale[0:1], 0.0)
        if i == 0:
            scale_ref[0] = scale
        else:
            scale_stage[i] = scale
            sc_copy(i).start()

    for copy in weight_copies:
        copy.wait()
    step_rows = min(256, units)

    def turn(i, carry):
        at = pl.ds(pl.multiple_of(i * step_rows, LANES), step_rows)
        down_t[:, at] = down_v[at, :].T
        return carry

    lax.fori_loop(0, units // step_rows, turn, 0)

    def turn_wide(i, carry):
        at = pl.ds(pl.multiple_of(i * span, LANES), span)
        gate_t[:, at] = gate_v[at, :].T
        up_t[:, at] = up_v[at, :].T
        return carry

    lax.fori_loop(0, width // span, turn_wide, 0)

    def y_copy(a, i, y_to):
        ref = outs[a].at[i, pl.ds(0, sent), cols(tp)]
        return remote(ref, ref, y_send.at[a, i, y_to], y_recv.at[a, i, y_at], {"tp": y_to * 2 + core})

    def y_arrival(a, i, y_from):
        ref = outs[a].at[i, pl.ds(0, sent), cols(y_from * 2 + core)]
        return remote(ref, ref, y_send.at[a, i, y_from], y_recv.at[a, i, y_from], {"tp": y_from * 2 + core})

    def p_copy(a, i, y_of):
        ref = outs[a].at[i, pl.ds(0, sent), cols(y_of * 2 + core)]
        return remote(ref, ref, p_send.at[a, i, y_of], p_recv.at[a, i, y_of], {"tp": partner})

    def p_arrival(a, i, y_of):
        ref = outs[a].at[i, pl.ds(0, sent), cols(y_of * 2 + 1 - core)]
        return remote(ref, ref, p_send.at[a, i, y_of], p_recv.at[a, i, y_of], {"tp": partner})

    def members(j):
        return [i for i in range(j * per, (j + 1) * per) if i > 0]

    def arrive(j):
        for i in members(j):
            for a in range(2):
                a_copy(a, i).wait_recv()
                for y_to in others_y:
                    y_copy(a, i, y_to).start()
                p_copy(a, i, y_at).start()

    def relay(j):
        for i in members(j):
            for a in range(2):
                for y_from in others_y:
                    y_arrival(a, i, y_from).wait_recv()
                    p_copy(a, i, y_from).start()

    def ready(j, a):
        for i in members(j):
            for y_of in [y_at] + others_y:
                p_arrival(a, i, y_of).wait_recv()

    def compute(j):
        at = slice(j * rows, (j + 1) * rows)
        for i in members(j):
            sc_copy(i).wait_recv()
        scale = scale_ref[j * per]
        for i in range(j * per + 1, (j + 1) * per):
            scale = scale + scale_ref[i]
        scale = jnp.broadcast_to(scale, (8, rows)).T[:, 0:1]
        ready(j, 0)
        x = x_ref[j * per : (j + 1) * per].reshape(rows, width)
        pre_gate = jnp.dot(x, gate_v[...], preferred_element_type=F32)
        pre_up = jnp.dot(x, up_v[...], preferred_element_type=F32)
        xt_ref[:, at] = x.T
        ready(j, 1)
        z = z_ref[j * per : (j + 1) * per].reshape(rows, width)
        back_proj = jnp.dot(z, down_t[...], preferred_element_type=F32)
        sig = jax.nn.sigmoid(pre_gate)
        hidden = (pre_gate * sig * pre_up).astype(BF16)
        terms = lane_sum(hidden.astype(F32) * back_proj)
        term_ref[j] = jnp.sum(terms.T, axis=0, keepdims=True)
        scaled = scale * back_proj
        grad_up = (scaled * pre_gate * sig).astype(BF16)
        grad_gate = (scaled * pre_up * sig * (1.0 + pre_gate * (1.0 - sig))).astype(BF16)
        up_pre_ref[at, :] = grad_up
        gate_pre_ref[at, :] = grad_gate
        part_span = min(width, 4 * LANES)
        for c in range(0, width, part_span):
            part = jnp.dot(grad_gate, gate_t[:, c : c + part_span], preferred_element_type=F32)
            part = part + jnp.dot(grad_up, up_t[:, c : c + part_span], preferred_element_type=F32)
            part_ref[j * per : (j + 1) * per, :, c : c + part_span] = (
                part.astype(BF16).reshape(per, slab, part_span)
            )
        ht_ref[:, at] = hidden.T
        weighted_ref[at, :] = (scale * z.astype(F32)).astype(BF16)

    def group(j):
        return pl.ds(j * per, per)

    def first(j, y_to):
        return remote(
            part_ref.at[group(j), pl.ds(0, sent), cols(y_to * 2 + 1 - core)], r1.at[y_to, group(j)],
            s1_send.at[j, y_to], s1_recv.at[j, y_to], {"tp": partner},
        )

    def second(j, y_to, y_from):
        return remote(
            s1.at[y_to, group(j)], r2.at[y_from, group(j)],
            s2_send.at[j, y_to], s2_recv.at[j, y_from], {"tp": y_to * 2 + core},
        )

    def third(i):
        return remote(
            res.at[i], back.at[i, pl.ds(0, sent)], s3_send.at[i], s3_recv.at[i], {"ep": peers[i]}
        )

    def gate_part(other, slot):
        return remote(term_ref, gate_in.at[slot], gt_send.at[other], gt_recv.at[slot], {"tp": other})

    def gate_home(i):
        return remote(
            gate_sum.at[i // per], gate_back.at[i], gb_send.at[i], gb_recv.at[i], {"ep": peers[i]}
        )

    def squares(other, slot):
        return remote(rowsq_ref, rowsq_in.at[slot], rs_send.at[other], rs_recv.at[slot], {"tp": other})

    def start_return(j):
        for y_to in others_y + [y_at]:
            first(j, y_to).start()

    def reduce_core(j):
        for y_to in others_y + [y_at]:
            first(j, y_to).wait_recv()
            mine = part_ref[j * per : (j + 1) * per, :sent, cols(y_to * 2 + core)].astype(F32)
            s1[y_to, group(j)] = (mine + r1[y_to, group(j)].astype(F32)).astype(BF16)
        for y_to in others_y:
            second(j, y_to, y_at).start()

    def reduce_y(j):
        value = s1[y_at, group(j)].astype(F32)
        for y_from in others_y:
            second(j, y_from, y_from).wait_recv()
            value = value + r2[y_from, group(j)].astype(F32)
        res[group(j)] = value.astype(BF16)
        for i in members(j):
            third(i).start()
        if j == 0:
            back[0, :sent] = res[0]

    arrive(0)
    for j in range(n_batch):
        if j + 1 < n_batch:
            arrive(j + 1)
        relay(j)
        compute(j)
        start_return(j)
        if j > 0:
            reduce_core(j - 1)
        if j > 1:
            reduce_y(j - 2)
    last = n_batch - 1
    for other in others_tp:
        gate_part(other, tp).start()

    def grads(c, carry):
        at = pl.ds(pl.multiple_of(c * span, LANES), span)
        xt = xt_ref[at, :]
        for a, (pre, out) in enumerate(((gate_pre_ref, gate_out), (up_pre_ref, up_out))):
            grad = jnp.dot(xt, pre[...], preferred_element_type=F32)
            out[at, :] = grad.astype(BF16)
            rowsq_ref[a, :, at] = jnp.sum(lane_sum(grad * grad).T, axis=0, keepdims=True)
        grad = jnp.dot(ht_ref[...], weighted_ref[:, at], preferred_element_type=F32)
        down_out[:, at] = grad.astype(BF16)
        down_acc[...] += lane_sum(grad * grad)
        return carry

    down_acc[...] = jnp.zeros_like(down_acc)
    chunks = width // span
    cut = [chunks * k // 4 for k in range(5)]
    lax.fori_loop(cut[0], cut[1], grads, 0)
    if n_batch > 1:
        reduce_y(last - 1)
    reduce_core(last)
    gate = term_ref[...]
    for other in others_tp:
        gate_part(other, other).wait_recv()
        gate = gate + gate_in[other]
    gate_sum[...] = gate
    for i in range(1, n_ep):
        gate_home(i).start()
    lax.fori_loop(cut[1], cut[2], grads, 0)
    reduce_y(last)
    lax.fori_loop(cut[2], cut[4], grads, 0)
    for other in others_tp:
        squares(other, tp).start()
    down_rows_ref[...] = jnp.sum(down_acc[...].T, axis=0, keepdims=True)

    d_weights = jnp.zeros((experts, tok_count), F32)
    for i in range(n_ep):
        if i == 0:
            terms = gate_sum[0]
        else:
            gate_home(i).wait_recv()
            terms = gate_back[i]
        terms = jnp.where(mine_of(i), terms, 0.0)
        terms = jnp.broadcast_to(terms, (experts, rows)).astype(BF16)
        found = jnp.dot(terms, pick_ref[i // per], preferred_element_type=F32)
        d_weights = jnp.where(expert_ids == peers[i], found, d_weights)
    mean = jnp.sum(d_weights * weights, axis=0, keepdims=True)
    d_logits = ((d_weights - mean) / total * aff * (1.0 - aff) * named).astype(BF16)
    rpart[...] = jnp.dot(d_logits, tok_ref[:, cols(tp)], preferred_element_type=F32)

    def router_copy(i):
        return remote(rpart, rparts.at[i], rp_send.at[i], rp_recv.at[i], {"ep": peers[i]})

    for i in range(1, n_ep):
        router_copy(i).start()

    grad = lax.dot_general(d_logits, router_ref[:, cols(tp)], ROWS_T, preferred_element_type=F32)
    for j in range(n_batch):
        for i in members(j):
            third(i).wait_recv()
        home = back[j * per : (j + 1) * per].reshape(rows, col_width)
        grad = grad + lax.dot_general(pick_ref[j], home, ROWS_T, preferred_element_type=F32)
    grad = grad.astype(BF16)
    tgrad[...] = grad
    token_ref[:, cols(tp)] = grad

    def to_y(y_to):
        return remote(
            tgrad, token_ref.at[:, cols(tp)], ty_send.at[y_to], ty_recv.at[y_at], {"tp": y_to * 2 + core}
        )

    def from_y(y_from):
        ref = token_ref.at[:, cols(y_from * 2 + core)]
        return remote(ref, ref, ty_send.at[y_from], ty_recv.at[y_from], {"tp": y_from * 2 + core})

    def own_pair():
        return remote(
            tgrad, token_ref.at[:, cols(tp)], tp_send.at[y_at], tp_recv.at[y_at], {"tp": partner}
        )

    def pair(y_of):
        ref = token_ref.at[:, cols(y_of * 2 + core)]
        return remote(ref, ref, tp_send.at[y_of], tp_recv.at[y_of], {"tp": partner})

    def pair_in(y_of):
        ref = token_ref.at[:, cols(y_of * 2 + 1 - core)]
        return remote(ref, ref, tp_send.at[y_of], tp_recv.at[y_of], {"tp": partner})

    for y_to in others_y:
        to_y(y_to).start()
    own_pair().start()

    rgrad = rpart[...]
    for i in range(1, n_ep):
        router_copy(i).wait_recv()
        rgrad = rgrad + rparts[i]
    rgrad_ref[...] = rgrad
    sums = rowsq_ref[...]
    for other in others_tp:
        squares(other, other).wait_recv()
        sums = sums + rowsq_in[other]
    rowsum_ref[...] = sums

    for y_from in others_y:
        from_y(y_from).wait_recv()
        pair(y_from).start()
    for y_of in [y_at] + others_y:
        pair_in(y_of).wait_recv()
    own_pair().wait_send()
    for other in others_y:
        to_y(other).wait_send()
        pair(other).wait_send()
    for other in others_tp:
        gate_part(other, tp).wait_send()
        squares(other, tp).wait_send()
    for i in range(1, n_ep):
        sc_copy(i).wait_send()
        for a in range(2):
            a_copy(a, i).wait_send()
            for y_to in others_y:
                y_copy(a, i, y_to).wait_send()
                p_copy(a, i, y_to).wait_send()
            p_copy(a, i, y_at).wait_send()
        gate_home(i).wait_send()
        third(i).wait_send()
        router_copy(i).wait_send()
    for j in range(n_batch):
        for y_to in others_y:
            first(j, y_to).wait_send()
            second(j, y_to, y_at).wait_send()
        first(j, y_at).wait_send()


def finish_kernel(
    token_ref, router_ref, sums_ref, gate_ref, up_ref, down_ref, down_rows_ref,
    token_out, router_out, rows_out, gate_rows, up_rows, gate_out, up_out, down_out, down_rows_out, sems,
):
    copies = [
        pltpu.make_async_copy(src, dst, sems.at[n])
        for n, (src, dst) in enumerate(
            ((gate_ref, gate_out), (up_ref, up_out), (down_ref, down_out), (token_ref, token_out))
        )
    ]
    for copy in copies:
        copy.start()
    grad = router_ref[...]
    router_out[...] = grad
    rows_out[...] = jnp.sum(grad * grad, axis=0, keepdims=True)
    gate_rows[...] = sums_ref[0]
    up_rows[...] = sums_ref[1]
    down_rows_out[...] = down_rows_ref[...]
    for copy in copies:
        copy.wait()


def per_device(tokens, routing, router_weight, gate_weight, up_weight, down_weight, cotangent):
    n_ep = lax.axis_size("ep")
    n_tp = lax.axis_size("tp")
    tok_count, width = tokens.shape
    top_count = routing.shape[1]
    experts = router_weight.shape[1]
    units = gate_weight.shape[2]
    capacity = 7 * tok_count * top_count // (4 * experts)
    sent = -(-capacity // 8) * 8
    slab = -(-capacity // 16) * 16
    col_width = width // n_tp
    n_batch = min(n_ep, 4)
    n_y = n_tp // 2
    rows = n_ep // n_batch * slab
    slots = n_ep * slab
    span = 2 * LANES if width % (2 * LANES) == 0 else LANES
    dims = (n_ep, n_tp, n_batch, sent, slab, col_width, span)
    vmem = pl.BlockSpec(memory_space=pltpu.VMEM)
    hbm = pl.BlockSpec(memory_space=pltpu.HBM)
    dma = pltpu.SemaphoreType.DMA
    on_chip = pltpu.VMEM

    results = pl.pallas_call(
        functools.partial(moe_kernel, dims),
        out_shape=(
            on_chip((tok_count, width), BF16),
            on_chip((experts, col_width), F32),
            on_chip((2, 1, width), F32),
            on_chip((width, units), BF16),
            on_chip((width, units), BF16),
            on_chip((units, width), BF16),
            on_chip((1, units), F32),
        ),
        in_specs=[vmem] * 4 + [hbm] * 3,
        out_specs=(vmem,) * 7,
        scratch_shapes=[
            pltpu.VMEM((n_ep, slab, width), BF16),
            pltpu.VMEM((n_ep, slab, width), BF16),
            pltpu.VMEM((n_ep, 1, rows), F32),
            pltpu.VMEM((width, units), BF16),
            pltpu.VMEM((width, units), BF16),
            pltpu.VMEM((units, width), BF16),
            pltpu.VMEM((units, width), BF16),
            pltpu.VMEM((units, width), BF16),
            pltpu.VMEM((width, units), BF16),
            dma((3,)),
            pltpu.VMEM((2, n_ep, slab, col_width), BF16),
            pltpu.VMEM((n_ep, 1, rows), F32),
            pltpu.VMEM((n_batch, rows, tok_count), BF16),
            pltpu.VMEM((experts, tok_count), F32),
            pltpu.VMEM((experts, tok_count), F32),
            pltpu.VMEM((width, slots), BF16),
            pltpu.VMEM((units, slots), BF16),
            pltpu.VMEM((slots, width), BF16),
            pltpu.VMEM((slots, units), BF16),
            pltpu.VMEM((slots, units), BF16),
            pltpu.VMEM((n_ep, slab, width), BF16),
            pltpu.VMEM((n_batch, 1, rows), F32),
            pltpu.VMEM((units, LANES), F32),
            pltpu.VMEM((n_y, n_ep, sent, col_width), BF16),
            pltpu.VMEM((n_y, n_ep, sent, col_width), BF16),
            pltpu.VMEM((n_y, n_ep, sent, col_width), BF16),
            pltpu.VMEM((n_ep, sent, col_width), BF16),
            pltpu.VMEM((n_ep, slab, col_width), BF16),
            pltpu.VMEM((n_tp, n_batch, 1, rows), F32),
            pltpu.VMEM((n_batch, 1, rows), F32),
            pltpu.VMEM((n_ep, 1, rows), F32),
            pltpu.VMEM((2, 1, width), F32),
            pltpu.VMEM((n_tp, 2, 1, width), F32),
            pltpu.VMEM((experts, col_width), F32),
            pltpu.VMEM((n_ep, experts, col_width), F32),
            pltpu.VMEM((tok_count, col_width), BF16),
            dma((n_ep,)), dma((n_ep,)),
            dma((2, n_ep)), dma((2, n_ep)),
            dma((2, n_ep, n_y)), dma((2, n_ep, n_y)),
            dma((2, n_ep, n_y)), dma((2, n_ep, n_y)),
            dma((n_batch, n_y)), dma((n_batch, n_y)),
            dma((n_batch, n_y)), dma((n_batch, n_y)),
            dma((n_ep,)), dma((n_ep,)),
            dma((n_tp,)), dma((n_tp,)),
            dma((n_ep,)), dma((n_ep,)),
            dma((n_tp,)), dma((n_tp,)),
            dma((n_ep,)), dma((n_ep,)),
            dma((n_y,)), dma((n_y,)),
            dma((n_y,)), dma((n_y,)),
        ],
        compiler_params=pltpu.CompilerParams(
            collective_id=0, has_side_effects=True, vmem_limit_bytes=48 << 20
        ),
        name="moe",
    )(tokens, cotangent, routing.T, router_weight.T, gate_weight, up_weight, down_weight)

    (token_grad, router_grad, router_rows, gate_rows, up_rows, grad_gate, grad_up, grad_down,
     down_rows) = pl.pallas_call(
        finish_kernel,
        out_shape=(
            jax.ShapeDtypeStruct((tok_count, width), BF16),
            jax.ShapeDtypeStruct((experts, col_width), F32),
            jax.ShapeDtypeStruct((1, col_width), F32),
            jax.ShapeDtypeStruct((1, width), F32),
            jax.ShapeDtypeStruct((1, width), F32),
            jax.ShapeDtypeStruct((width, units), BF16),
            jax.ShapeDtypeStruct((width, units), BF16),
            jax.ShapeDtypeStruct((units, width), BF16),
            jax.ShapeDtypeStruct((1, units), F32),
        ),
        in_specs=[vmem] * 7,
        out_specs=(hbm, vmem, vmem, vmem, vmem, hbm, hbm, hbm, vmem),
        scratch_shapes=[dma((4,))],
        compiler_params=pltpu.CompilerParams(vmem_limit_bytes=16 << 20),
        name="finish",
    )(*results)
    return (
        token_grad,
        router_grad.T,
        router_rows[0],
        grad_gate[None],
        grad_up[None],
        grad_down[None],
        gate_rows,
        up_rows,
        down_rows,
    )


def solution(mesh):
    return jax.shard_map(
        per_device,
        mesh=mesh,
        in_specs=(
            P("ep", None),
            P("ep", None),
            P(),
            P("ep", None, "tp"),
            P("ep", None, "tp"),
            P("ep", "tp", None),
            P("ep", None),
        ),
        out_specs=(
            P("ep", None),
            P("tp", None),
            P("tp"),
            P("ep", None, "tp"),
            P("ep", None, "tp"),
            P("ep", "tp", None),
            P("ep", None),
            P("ep", None),
            P("ep", "tp"),
        ),
        check_vma=False,
    )
```

time: 98.8 us -> 66.5 us (0.67); the launches traced: 97.2 us -> 66.1 us
  Pallas kernels: 96.5 us -> 65.4 us
    pallas_call x3 -> x1, Pallas kernels: 94.6 us -> 62 us  [per_device(): pl.pallas_call(functools.partial(moe_kernel, dims), out_shape=(on_chip((t...]
    pallas_call x1, Pallas kernels: 1.9 us -> 3.46 us  [per_device(): pl.pallas_call(finish_kernel, out_shape=(jax.ShapeDtypeStruct((tok_count,...]
where the time goes in v1:
time: 66.5 us; the launch traced here: 66.1 us
  Pallas kernels  65.4 us (98%)
    pallas_call x1, Pallas kernels, per_device(): pl.pallas_call(functools.partial(moe_kernel, dims), out_shape=(on_chip((t...  62 us
    pallas_call x1, Pallas kernels, per_device(): pl.pallas_call(finish_kernel, out_shape=(jax.ShapeDtypeStruct((tok_count,...  3.46 us

profile of v1, /device:TPU:0, one launch (start us, length us, event | category | flops | bytes accessed | tf_op | source)
XLA Modules:
  0.0 66.1 jit_solution(5571760187710923685)
XLA Ops:
  0.6 62.0 %moe.1 = (bf16[128,2048]{1,0:T(8,128)(2,1)S(1)}, f32[8,512]{1,0:T(8,128)S(1)}, f32[2,1,2048]{2,1,0:T(1,128)S(1)}, bf16[2048,512]{1,0:T(8,128)(2,1)S(1)}, bf16[20...) custom-call(bf16[128,2048]{1,0:T(8,128)(2,1)} %tok_ref.1, bf16[128,2048]{1,0:T(8,128)(2,1)} %cot_ref.1, ...), custom_call_target="tpu_custom_call" | custom-call | tf_op jit(solution)/shard_map/moe/pallas_call | solution.py:494
  62.6 3.5 %finish.1 = (bf16[128,2048]{1,0:T(8,128)(2,1)}, f32[8,512]{1,0:T(8,128)}, f32[1,512]{1,0:T(1,128)}, f32[1,2048]{1,0:T(1,128)}, f32[1,2048]{1,0:T(1,128)}, /*inde...) custom-call(bf16[128,2048]{1,0:T(8,128)(2,1)S(1)} %get-tuple-element.25.token_ref, ...), custom_call_target="tpu_custom_call" | custom-call | tf_op jit(solution)/shard_map/finish/pallas_call | solution.py:565
